TPU v7x, 32 devices: a whole 2x2x4 slice. The times are simulated.
32 devices in a mesh: sp: 8 (over z, y), tp: 4 (over x, core).
Axes of the slice: x: 2, y: 2, z: 4, core: 2. Of those that a mesh axis runs over, the one named last changes fastest.
Arguments:
- query_one: bfloat16 [2048, 512], P('sp', 'tp'), may hold values from -190 to 190
- query_two: bfloat16 [2048, 512], P('sp', 'tp'), may hold values from -190 to 190
- key_one: bfloat16 [2048, 512], P('sp', 'tp'), may hold values from -10 to 10
- key_two: bfloat16 [2048, 512], P('sp', 'tp'), may hold values from -10 to 10
- values: bfloat16 [2048, 1024], P('sp', 'tp'), may hold values from -6 to 6
- mix_lambda: float32 [8], P('tp'), may hold values from 0.3 to 0.8
- head_gain: float32 [128], replicated, may hold values from 0.1 to 1.9
- stream: bfloat16 [2048, 2048], P('sp', 'tp'), may hold values from -6 to 6
- out_weight: bfloat16 [1024, 2048], P('tp'), may hold values from -0.1875 to 0.1875
- first_gain: float32 [2048], replicated, may hold values from 0.1 to 1.9
- up_weight: bfloat16 [2048, 4096], P('sp', 'tp'), may hold values from -0.125 to 0.125
- down_weight: bfloat16 [4096, 2048], P('tp', 'sp'), may hold values from -0.09375 to 0.09375
- second_gain: float32 [2048], replicated, may hold values from 0.1 to 1.9
Outputs:
- layer_out: bfloat16 [2048, 2048], P(('sp', 'tp'))
All inputs are finite; a program needn't handle non-finite values.
Results may differ from a plain program's by a relative error of at most 0.019.
Values may be sent and summed in bfloat16 or wider, within the bound.
A program may use at most 128 MiB of HBM per device.

v0:
```python
import math

import jax
import jax.numpy as jnp
from jax import lax
from jax.sharding import PartitionSpec as P

alpha_mix = 2.0**0.5


def layer_norm(value, gain):
    centre = jnp.mean(value, axis=-1, keepdims=True)
    spread = jnp.mean(jnp.square(value - centre), axis=-1, keepdims=True)
    return (value - centre) * lax.rsqrt(spread + 1e-05) * gain


def absorb_map(run_max, run_sum, run_acc, queries, keys, vals, scale):
    scores = jnp.einsum("qhd,khd->hqk", queries, keys, preferred_element_type=jnp.float32) * scale
    new_max = jnp.maximum(run_max, jnp.max(scores, axis=-1))
    factor = jnp.exp(run_max - new_max)
    expo = jnp.exp(scores - new_max[..., None])
    run_sum = run_sum * factor + jnp.sum(expo, axis=-1)
    run_acc = run_acc * factor[..., None] + jnp.einsum(
        "hqk,khe->hqe", expo.astype(jnp.bfloat16), vals, preferred_element_type=jnp.float32
    )
    return (new_max, run_sum, run_acc)


def local(
    query_one,
    query_two,
    key_one,
    key_two,
    values,
    mix_lambda,
    head_gain,
    stream,
    out_weight,
    first_gain,
    up_weight,
    down_weight,
    second_gain,
):
    tokens = query_one.shape[0]
    heads_local = mix_lambda.shape[0]
    qk_width = query_one.shape[1] // heads_local
    v_width = values.shape[1] // heads_local
    scale = qk_width ** (-0.5)
    queries_a = query_one.reshape(tokens, heads_local, qk_width)
    queries_b = query_two.reshape(tokens, heads_local, qk_width)
    lowest = jnp.full((heads_local, tokens), -1e30, jnp.float32)
    zero_sum = jnp.zeros((heads_local, tokens), jnp.float32)
    zero_acc = jnp.zeros((heads_local, tokens, v_width), jnp.float32)
    pieces = (
        lax.all_gather(key_one, "sp", axis=0, tiled=True),
        lax.all_gather(key_two, "sp", axis=0, tiled=True),
        lax.all_gather(values, "sp", axis=0, tiled=True),
    )
    count = pieces[0].shape[0]
    block = math.gcd(count, 1024)
    nblk = count // block
    keys_a = pieces[0].reshape(nblk, block, heads_local, qk_width)
    keys_b = pieces[1].reshape(nblk, block, heads_local, qk_width)
    vals = pieces[2].reshape(nblk, block, heads_local, v_width)

    def step(carry, inputs):
        max_a, sum_a, acc_a, max_b, sum_b, acc_b = carry
        max_a, sum_a, acc_a = absorb_map(
            max_a, sum_a, acc_a, queries_a, inputs[0], inputs[2], scale
        )
        max_b, sum_b, acc_b = absorb_map(
            max_b, sum_b, acc_b, queries_b, inputs[1], inputs[2], scale
        )
        return ((max_a, sum_a, acc_a, max_b, sum_b, acc_b), None)

    result, _ = lax.scan(
        step, (lowest, zero_sum, zero_acc, lowest, zero_sum, zero_acc), (keys_a, keys_b, vals)
    )
    max_a, sum_a, acc_a, max_b, sum_b, acc_b = result
    mixed = acc_a / sum_a[..., None] - mix_lambda[:, None, None] * acc_b / sum_b[..., None]
    normed = (
        mixed
        * lax.rsqrt(jnp.mean(jnp.square(mixed), axis=-1, keepdims=True) + 1e-05)
        * head_gain
        * 0.8
    )
    attended = jnp.transpose(normed.astype(jnp.bfloat16), (1, 0, 2)).reshape(
        tokens, heads_local * v_width
    )
    tp_index = lax.axis_index("tp")
    own_cols = stream.shape[1]
    col_start = tp_index * own_cols
    share = tokens // lax.axis_size("tp")
    row_start = tp_index * share
    partial_rows = jnp.dot(attended, out_weight, preferred_element_type=jnp.float32)
    own = lax.dynamic_slice_in_dim(partial_rows, col_start, own_cols, 1)
    own = own + alpha_mix * stream.astype(jnp.float32)
    pre = lax.psum(
        lax.dynamic_update_slice_in_dim(partial_rows, own, col_start, 1).astype(jnp.bfloat16), "tp"
    ).astype(jnp.float32)
    hidden_in = layer_norm(pre, first_gain).astype(jnp.bfloat16)
    up_full, down_full = (
        lax.all_gather(up_weight, "sp", axis=0, tiled=True),
        lax.all_gather(down_weight, "sp", axis=1, tiled=True),
    )
    upper = jnp.dot(hidden_in, up_full, preferred_element_type=jnp.float32)
    act = jnp.square(jax.nn.relu(upper)).astype(jnp.bfloat16)
    post = lax.psum_scatter(
        jnp.dot(act, down_full, preferred_element_type=jnp.float32).astype(jnp.bfloat16),
        "tp",
        scatter_dimension=0,
        tiled=True,
    ).astype(jnp.float32)
    post = post + alpha_mix * lax.dynamic_slice_in_dim(hidden_in, row_start, share, 0).astype(
        jnp.float32
    )
    return layer_norm(post, second_gain).astype(jnp.bfloat16)


def solution(mesh):
    in_specs = (
        P("sp", "tp"),
        P("sp", "tp"),
        P("sp", "tp"),
        P("sp", "tp"),
        P("sp", "tp"),
        P("tp"),
        P(),
        P("sp", "tp"),
        P("tp", None),
        P(),
        P("sp", "tp"),
        P("tp", "sp"),
        P(),
    )
    out_specs = P(("sp", "tp"), None)
    return jax.shard_map(local, mesh=mesh, in_specs=in_specs, out_specs=out_specs, check_vma=False)
```

profile of v0, /device:TPU:0, one launch (start us, length us, event | category | flops | bytes accessed | tf_op | source)
XLA Modules:
  0.0 321.0 jit_solution(10274457005820370710)
XLA Ops:
  6.5 0.0 copy-start
  6.5 0.0 all-gather.4.cloned.1.call-start
  6.5 0.7 all-gather.4.cloned.1.call-update
  7.3 0.0 all-reduce.2.cloned.1.call-start
  7.4 33.7 %all_gather.15 = bf16[2048,128]{1,0:T(8,128)(2,1)S(1)} all-gather(bf16[256,128]{1,0:T(8,128)(2,1)} %param.17), channel_id=1, replica_groups=mesh['sp'=8,'tp'=4] {'sp'}, dimensions={0}, use_global_device_ids=true | all-gather | bytes 589824 | tf_op jit(solution)/shard_map/all_gather | solution.py:55
  41.1 0.4 reshape.66
  41.5 0.7 copy.24
  42.2 0.0 copy-done.4
  42.2 0.0 copy-start.5
  42.2 0.0 copy-start.6
  42.3 34.0 %all_gather.17 = bf16[2048,128]{1,0:T(8,128)(2,1)} all-gather(bf16[256,128]{1,0:T(8,128)(2,1)S(1)} %copy-done.4), channel_id=1, replica_groups=mesh['sp'=8,'tp'=4] {'sp'}, dimensions={0}, use_global_device_ids=true | all-gather | bytes 589824 | tf_op jit(solution)/shard_map/all_gather | solution.py:56
  76.3 2.4 reshape.67
  78.7 1.9 copy.26
  80.7 0.0 copy-done.5
  80.7 0.1 copy.21
  80.8 0.1 copy.23
  80.9 0.0 all-gather.4.cloned.1.call-done
  80.9 1.3 reshape.62
  82.3 0.0 copy-start.10
  82.3 0.0 copy-start.9
  82.3 7.5 %while.21 = (s32[]{:T(128)}, f32[2,256]{1,0:T(2,128)S(1)}, f32[2,256]{1,0:T(2,128)S(1)}, f32[2,256,128]{2,1,0:T(8,128)S(1)}, f32[2,256]{1,0:T(2,128)S(1)}, /*ind...) while((s32[]{:T(128)}, f32[2,256]{1,0:T(2,128)S(1)}, ...), condition=%wide.region_5.6_spmd.clone, body=%wide.region_0.5_spmd.clone.sunk | while | flops 411440128 | bytes 18546876 | solution.py:76
  82.3 0.5 bitcast_reduce_fusion.4
  82.9 0.4 fusion.60
  83.2 0.1 copy-done.2
  83.4 0.5 bitcast_reduce_fusion.5
  83.9 0.4 fusion.59
  84.3 0.4 constant_dynamic-slice_fusion.2
  84.7 0.7 convolution_add_fusion.5
  85.4 0.7 convolution_add_fusion.4
  86.1 0.5 bitcast_reduce_fusion.4
  86.6 0.4 fusion.60
  87.0 0.2 copy-done.2
  87.1 0.5 bitcast_reduce_fusion.5
  87.6 0.4 fusion.59
  88.0 0.4 constant_dynamic-slice_fusion.2
  88.4 0.7 convolution_add_fusion.5
  89.1 0.7 convolution_add_fusion.4
  89.8 0.1 copy.27
  90.0 0.1 copy.28
  90.1 0.0 copy-start.3
  90.1 0.1 multiply_reduce_fusion.1
  90.3 0.1 multiply_convert_fusion.1
  90.4 0.5 fusion.36
  90.8 0.2 copy-done.3
  91.1 0.1 add_dynamic-update-slice_fusion
  91.2 1.1 convert_element_type.38
  92.3 0.0 all-reduce.2.cloned.1.call-update
  92.3 0.0 all-gather.6.cloned.1.call-start
  92.4 0.7 all-gather.6.cloned.1.call-update
  93.1 0.0 all-gather.8.cloned.1.call-start
  93.1 0.5 all-gather.8.cloned.1.call-update
  93.6 0.0 reduce-scatter.2.cloned.1.call-start
  93.7 36.1 %all-reduce.2.cloned.1.call-done = bf16[256,2048]{1,0:T(8,128)(2,1)} async-done(((bf16[256,2048]{1,0:T(8,128)(2,1)}), bf16[256,2048]{1,0:T(8,128)(2,1)}) %all-reduce.2.cloned.1.call-update) | async-done | bytes 1048592 | tf_op jit(solution)/shard_map/psum | solution.py:98
  129.8 1.5 convert_reduce_fusion
  131.3 1.6 fusion.28
  133.0 0.4 fusion.30
  133.4 71.8 %all-gather.6.cloned.1.call-done = bf16[2048,1024]{1,0:T(8,128)(2,1)} async-done(((bf16[256,1024]{1,0:T(8,128)(2,1)}), bf16[2048,1024]{1,0:T(8,128)(2,1)}) %all-gather.6.cloned.1.call-update) | async-done | bytes 4194320 | tf_op jit(solution)/shard_map/all_gather | solution.py:103
  205.2 75.1 %all-gather.8.cloned.1.call-done = bf16[1024,2048]{1,0:T(8,128)(2,1)} async-done(((bf16[1024,256]{1,0:T(8,128)(2,1)}), bf16[1024,2048]{1,0:T(8,128)(2,1)}) %all-gather.8.cloned.1.call-update) | async-done | bytes 4194320 | tf_op jit(solution)/shard_map/all_gather | solution.py:104
  280.3 6.9 %convolution_convert_fusion = bf16[256,2048]{1,0:T(8,128)(2,1)} fusion(bf16[1024,2048]{1,0:T(8,128)(2,1)} %all-gather.8.cloned.1.call-done, bf16[256,2048]{1,0:T(8,128)(2,1)S(1)} %fusion.30, bf16[2048,1024]{1,0:T(8,128)(2,1)} %all-gather.6.cloned.1.call-done), kind=kOutput, calls=%fused_computation.42 | convolution fusion | flops 2148794368 | bytes 10485760 | tf_op jit(solution)/shard_map/dot_general | solution.py:109
  287.2 0.0 reduce-scatter.2.cloned.1.call-update
  287.2 23.1 %reduce-scatter.2.cloned.1.call-done = bf16[64,2048]{1,0:T(8,128)(2,1)} async-done(((bf16[256,2048]{1,0:T(8,128)(2,1)}), bf16[64,2048]{1,0:T(8,128)(2,1)}) %reduce-scatter.2.cloned.1.call-update) | async-done | bytes 262160 | tf_op jit(solution)/shard_map/reduce_scatter | solution.py:108
  310.3 1.1 fusion.34
  311.5 1.2 multiply_reduce_fusion
  312.7 1.8 multiply_convert_fusion
  (34 shorter events, 0.1 us)
Async XLA Ops:
  6.5 83.8 %copy-start = (bf16[256,2048]{1,0:T(8,128)(2,1)S(1)}, bf16[256,2048]{1,0:T(8,128)(2,1)}, u32[]{:S(2)}) copy-start(bf16[256,2048]{1,0:T(8,128)(2,1)} %param.23) | copy-start | bytes 3145732
  6.5 35.7 %copy-start.4 = (bf16[256,128]{1,0:T(8,128)(2,1)S(1)}, bf16[256,128]{1,0:T(8,128)(2,1)}, u32[]{:S(2)}) copy-start(bf16[256,128]{1,0:T(8,128)(2,1)} %param.18) | copy-start | bytes 196612
  6.5 74.4 %all-gather.4.cloned.1.call-start = ((), (), s32[]{:S(2)}) async-start(), calls=%async_computation.1 | async-start | bytes 1179648 | tf_op jit(solution)/shard_map/all_gather | solution.py:57
  7.3 122.5 %all-reduce.2.cloned.1.call-start = ((), (), s32[]{:S(2)}) async-start(), calls=%async_computation.2 | async-start | bytes 2097152 | tf_op jit(solution)/shard_map/psum | solution.py:98
  42.2 38.4 %copy-start.5 = (bf16[256,128]{1,0:T(8,128)(2,1)S(1)}, bf16[256,128]{1,0:T(8,128)(2,1)}, u32[]{:S(2)}) copy-start(bf16[256,128]{1,0:T(8,128)(2,1)} %param.15) | copy-start | bytes 196612
  42.2 38.5 %copy-start.6 = (bf16[256,128]{1,0:T(8,128)(2,1)S(1)}, bf16[256,128]{1,0:T(8,128)(2,1)}, u32[]{:S(2)}) copy-start(bf16[256,128]{1,0:T(8,128)(2,1)} %param.16) | copy-start | bytes 196612
  82.3 7.8 %copy-start.10 = (f32[2]{0:T(128)S(1)}, f32[2]{0:T(128)}, u32[]{:S(2)}) copy-start(f32[2]{0:T(128)} %param.20) | copy-start | bytes 28
  82.3 8.0 %copy-start.9 = (f32[128]{0:T(128)S(1)}, f32[128]{0:T(128)}, u32[]{:S(2)}) copy-start(f32[128]{0:T(128)} %param.21) | copy-start | bytes 1540
  82.3 1.0 copy-start.2
  86.1 1.0 copy-start.2
  90.1 1.0 copy-start.3
  92.3 40.7 %copy-start.7 = (f32[2048]{0:T(1024)S(1)}, f32[2048]{0:T(1024)}, u32[]{:S(2)}) copy-start(f32[2048]{0:T(1024)} %param.24) | copy-start | bytes 24580
  92.3 112.9 %all-gather.6.cloned.1.call-start = ((), (), s32[]{:S(2)}) async-start(), calls=%async_computation.3 | async-start | bytes 4718592 | tf_op jit(solution)/shard_map/all_gather | solution.py:103
  93.1 187.2 %all-gather.8.cloned.1.call-start = ((), (), s32[]{:S(2)}) async-start(), calls=%async_computation.4 | async-start | bytes 4718592 | tf_op jit(solution)/shard_map/all_gather | solution.py:104
  93.6 216.7 %reduce-scatter.2.cloned.1.call-start = ((), (), s32[]{:S(2)}) async-start(), calls=%async_computation.5 | async-start | bytes 1310720 | tf_op jit(solution)/shard_map/reduce_scatter | solution.py:108
  129.8 3.2 copy-start.1
  287.2 25.5 %copy-start.8 = (f32[2048]{0:T(1024)S(1)}, f32[2048]{0:T(1024)}, u32[]{:S(2)}) copy-start(f32[2048]{0:T(1024)} %param.27) | copy-start | bytes 24580
Sparse Core Ops, SparseCore 0:
  9.5 44.6 all-gather.3
  92.4 37.2 all-reduce.1
  131.9 73.2 all-gather.5
  207.1 73.1 all-gather.7
  287.3 22.9 reduce-scatter.1
where the time goes:
time: 321 us
  waiting for transfers between devices  208 us (65%)
  blocking collectives  67.7 us (21%)
  between operations  13.4 us (4%)
  matrix products  12.1 us (4%)
  other arithmetic  10.7 us (3%)
  local copies, waits for them, and re-layouts  8.66 us (3%)
    all_gather x1, waiting for transfers between devices, local(): lax.all_gather(down_weight, 'sp', axis=1, tiled=True)  75.1 us
    all_gather x1, waiting for transfers between devices, local(): lax.all_gather(up_weight, 'sp', axis=0, tiled=True)  71.8 us
    psum x1, waiting for transfers between devices, local(): lax.psum(lax.dynamic_update_slice_in_dim(partial_rows, own, col_start, 1)...  36.1 us
    all_gather x1, blocking collectives, local(): lax.all_gather(key_two, 'sp', axis=0, tiled=True)  34 us
    all_gather x1, blocking collectives, local(): lax.all_gather(key_one, 'sp', axis=0, tiled=True)  33.7 us
    reduce_scatter x1, waiting for transfers between devices, local(): lax.psum_scatter(jnp.dot(act, down_full, preferred_element_type=jnp.float...  23.1 us
    dot_general x1, matrix products, local(): jnp.dot(act, down_full, preferred_element_type=jnp.float32)  6.87 us
  transfers between devices with their start and end apart: 5, of which 4 were waited for; matrix products, arithmetic and copies ran while one was open for 3% of the time, Pallas kernels for 0%

commit v1 on v0

v1 whole, which is shorter than its diff:
```python
import functools
import math

import jax
import jax.numpy as jnp
from jax import lax
from jax.experimental import pallas as pl
from jax.experimental.pallas import tpu as pltpu
from jax.sharding import PartitionSpec as P

MESH = pl.DeviceIdType.MESH
F32, BF16 = jnp.float32, jnp.bfloat16
ALPHA = 2.0**0.5
NT = (((1,), (1,)), ((), ()))
TN = (((0,), (0,)), ((), ()))


def layer_norm(value, gain):
    centre = jnp.mean(value, axis=-1, keepdims=True)
    spread = jnp.mean(jnp.square(value - centre), axis=-1, keepdims=True)
    return (value - centre) * lax.rsqrt(spread + 1e-05) * gain


def kernel(
    nsp, ntp, heads,
    lam_ref, q1_ref, q2_ref, kv_ref, hg_ref, st_ref, ow_ref, g1_ref, up_ref, dn_ref, g2_ref,
    out_ref,
    qm, m_run, l_run, acc, kv_buf, up_buf, dn_buf, ow_buf, st_buf, at_snd, at_buf,
    pre, h_own, h_buf, act, sib_snd, sib_buf, part, red_snd, red_buf,
    loc_sem, kvz, kvy, upz, upy, dnz, dny, owx, ows, sts, ats, hps, hss, sbs, rds,
):
    s, t = lax.axis_index("sp"), lax.axis_index("tp")
    nz, nth = nsp // 2, ntp // 2
    ng = 2 * nth
    z, y = s // 2, s % 2
    zh, zl = z // 2, z % 2
    th, tl = t // 2, t % 2
    sib_t = th * 2 + (1 - tl)
    y_sp = z * 2 + (1 - y)
    grp = zl * nth + th
    tok = q1_ref.shape[0]
    share = tok // ntp
    fh = up_ref.shape[1] // 2
    kw = q1_ref.shape[1]
    qk = kw // heads
    vd = acc.shape[1]
    hv = heads * vd
    d = pre.shape[1]

    def rc(src, dst, sems, i, sp, tp):
        return pltpu.make_async_remote_copy(
            src_ref=src, dst_ref=dst, send_sem=sems.at[0, i], recv_sem=sems.at[1, i],
            device_id={"sp": sp, "tp": tp}, device_id_type=MESH,
        )

    def each(lo, hi, body):
        if hi - lo <= 4:
            for k in range(lo, hi):
                body(k)
        else:
            lax.fori_loop(lo, hi, lambda k, c: (body(k), c)[1], 0)

    def zto(k):
        return lax.rem(z + k, nz)

    def zfrom(k):
        return lax.rem(z + nz - k, nz)

    def kv_z(k):
        return rc(kv_ref, kv_buf.at[s], kvz, k, zto(k) * 2 + y, t)

    def kv_y0():
        return rc(kv_ref, kv_buf.at[s], kvy, 0, y_sp, t)

    def kv_y(k):
        b = zfrom(k) * 2 + y
        return rc(kv_buf.at[b], kv_buf.at[b], kvy, k, y_sp, t)

    def up_half(j):
        return up_ref.at[:, pl.ds(pl.multiple_of(j * fh, fh), fh)]

    def dn_half(j):
        return dn_ref.at[pl.ds(pl.multiple_of(j * fh, fh), fh), :]

    def up_z(k):
        zd = zto(k)
        return rc(up_half(zd % 2), up_buf.at[s], upz, k, zd * 2 + y, t)

    def dn_z(k):
        zd = zto(k)
        return rc(dn_half(zd % 2), dn_buf.at[s], dnz, k, zd * 2 + y, t)

    def up_y0():
        return rc(up_half(zl), up_buf.at[s], upy, 0, y_sp, t)

    def dn_y0():
        return rc(dn_half(zl), dn_buf.at[s], dny, 0, y_sp, t)

    def up_y(k):
        b = zfrom(k) * 2 + y
        return rc(up_buf.at[b], up_buf.at[b], upy, k, y_sp, t)

    def dn_y(k):
        b = zfrom(k) * 2 + y
        return rc(dn_buf.at[b], dn_buf.at[b], dny, k, y_sp, t)

    def ow_x(k):
        return rc(ow_ref, ow_buf.at[t], owx, k, s, lax.rem(th + k, nth) * 2 + tl)

    def ow_s0():
        return rc(ow_ref, ow_buf.at[t], ows, 0, s, sib_t)

    def ow_s(k):
        b = lax.rem(th + nth - k, nth) * 2 + tl
        return rc(ow_buf.at[b], ow_buf.at[b], ows, k, s, sib_t)

    def rows_of(tt):
        return pl.ds(pl.multiple_of(tt * share, share), share)

    def st_c(k):
        td = lax.rem(t + k, ntp)
        return rc(st_ref.at[rows_of(td), :], st_buf.at[t], sts, k, s, td)

    def at_c(k):
        td = lax.rem(t + k, ntp)
        return rc(at_snd.at[rows_of(td), :], at_buf.at[t], ats, k, s, td)

    def grp_dev(g):
        return (zh * 2 + g // nth) * 2 + y, lax.rem(g, nth) * 2 + tl

    def h_p(k):
        sp, tp = grp_dev(lax.rem(grp + k, ng))
        return rc(h_own, h_buf.at[tl, grp], hps, k, sp, tp)

    def h_s0():
        return rc(h_own, h_buf.at[tl, grp], hss, 0, s, sib_t)

    def h_s(k):
        g = lax.rem(grp + ng - k, ng)
        return rc(h_buf.at[tl, g], h_buf.at[tl, g], hss, k, s, sib_t)

    def sib_c():
        return rc(sib_snd, sib_buf, sbs, 0, s, sib_t)

    def red_c(k):
        g = lax.rem(grp + k, ng)
        sp, tp = grp_dev(g)
        return rc(red_snd.at[g], red_buf.at[grp], rds, k, sp, tp)

    barrier = pltpu.get_barrier_semaphore()

    def greet(sp, tp):
        pl.semaphore_signal(barrier, inc=1, device_id={"sp": sp, "tp": tp}, device_id_type=MESH)

    each(1, nz, lambda k: greet(zto(k) * 2 + y, t))
    greet(y_sp, t)
    each(1, ntp, lambda k: greet(s, lax.rem(t + k, ntp)))
    each(1, nth, lambda k: greet((zh * 2 + 1 - zl) * 2 + y, lax.rem(th + k, nth) * 2 + tl))
    pl.semaphore_wait(barrier, (nz - 1) + 1 + (ntp - 1) + (nth - 1))

    each(1, nz, lambda k: kv_z(k).start())
    kv_y0().start()
    each(1, ntp, lambda k: st_c(k).start())
    each(1, nth, lambda k: ow_x(k).start())
    ow_s0().start()
    locals_ = [
        pltpu.make_async_copy(ow_ref, ow_buf.at[t], loc_sem.at[0]),
        pltpu.make_async_copy(up_half(zl), up_buf.at[s], loc_sem.at[1]),
        pltpu.make_async_copy(dn_half(zl), dn_buf.at[s], loc_sem.at[2]),
    ]
    for c in locals_:
        c.start()
    each(1, nz, lambda k: up_z(k).start())
    each(1, nz, lambda k: dn_z(k).start())

    scale = qk ** (-0.5)
    lane = lax.broadcasted_iota(jnp.int32, (tok, kw), 1)
    for i, q_ref in enumerate((q1_ref, q2_ref)):
        qv = q_ref[...].astype(F32) * scale
        for h in range(heads):
            keep = (lane >= h * qk) & (lane < (h + 1) * qk)
            qm[i * heads + h] = jnp.where(keep, qv, 0.0).astype(BF16)
    m_run[...] = jnp.full(m_run.shape, -1e30, F32)
    l_run[...] = jnp.zeros(l_run.shape, F32)
    acc[...] = jnp.zeros(acc.shape, F32)

    def absorb(block):
        for h in range(heads):
            v = block[:, 2 * kw + h * vd : 2 * kw + (h + 1) * vd]
            for i in range(2):
                r = i * heads + h
                sc = lax.dot_general(
                    block[:, i * kw : (i + 1) * kw], qm[r], NT, preferred_element_type=F32
                )
                old = m_run[r]
                new = jnp.maximum(old, jnp.max(sc, axis=0, keepdims=True))
                fac = jnp.exp(old - new)
                ex = jnp.exp(sc - new)
                l_run[r] = l_run[r] * fac + jnp.sum(ex, axis=0, keepdims=True)
                acc[r] = acc[r] * fac + lax.dot_general(
                    v, ex.astype(BF16), TN, preferred_element_type=F32
                )
                m_run[r] = new

    absorb(kv_ref)

    def z_step(k, c):
        kv_z(k).wait_recv()
        kv_y(k).start()
        absorb(kv_buf.at[zfrom(k) * 2 + y])
        return c

    lax.fori_loop(1, nz, z_step, 0)
    up_y0().start()
    dn_y0().start()

    def y_step(k, c):
        kv_y(k).wait_recv()
        absorb(kv_buf.at[zfrom(k) * 2 + 1 - y])
        return c

    lax.fori_loop(0, nz, y_step, 0)

    for k in range(1, nth):
        ow_x(k).wait_recv()
        ow_s(k).start()

    for h in range(heads):
        mixed = acc[h] / l_run[h] - lam_ref[h] * (acc[heads + h] / l_run[heads + h])
        inv = lax.rsqrt(jnp.mean(jnp.square(mixed), axis=0, keepdims=True) + 1e-05)
        normed = jnp.transpose(mixed * inv) * hg_ref[...] * 0.8
        at_snd[:, h * vd : (h + 1) * vd] = normed.astype(BF16)
    each(1, ntp, lambda k: at_c(k).start())
    at_buf[t] = at_snd[rows_of(t), :]
    st_buf[t] = st_ref[rows_of(t), :]
    up_z(1).wait_recv()
    up_y(1).start()

    each(1, ntp, lambda k: st_c(k).wait_recv())
    cols = st_ref.shape[1]
    for b in range(ntp):
        pre[:, b * cols : (b + 1) * cols] = ALPHA * st_buf[b].astype(F32)
    locals_[0].wait()
    ow_s0().wait_recv()
    for k in range(1, nth):
        ow_s(k).wait_recv()
    each(1, ntp, lambda k: at_c(k).wait_recv())
    for b in range(ntp):
        pre[...] += jnp.dot(at_buf[b], ow_buf[b], preferred_element_type=F32)
    h_own[...] = layer_norm(pre[...], g1_ref[...]).astype(BF16)
    each(1, ng, lambda k: h_p(k).start())
    h_s0().start()
    h_buf[tl, grp] = h_own[...]

    def up_fwd(k):
        up_z(k).wait_recv()
        up_y(k).start()

    each(2, nz, up_fwd)

    def h_fwd(k):
        h_p(k).wait_recv()
        h_s(k).start()

    each(1, ng, h_fwd)

    def dn_fwd(k):
        dn_z(k).wait_recv()
        dn_y(k).start()

    each(1, nz, dn_fwd)
    h_s0().wait_recv()
    each(1, ng, lambda k: h_s(k).wait_recv())
    locals_[1].wait()
    up_y0().wait_recv()
    each(1, nz, lambda k: up_y(k).wait_recv())

    half = ng * share
    depth = up_buf.shape[1]
    for side in range(2):
        for c in range(2 if fh % 256 == 0 else 1):
            wide = fh // (2 if fh % 256 == 0 else 1)
            at = slice(c * wide, (c + 1) * wide)
            hid = h_buf[side].reshape(half, d)
            w = up_buf[:, :, at].reshape(d, wide)
            up = jnp.dot(hid, w, preferred_element_type=F32)
            act[side, :, at] = jnp.square(jnp.maximum(up, 0.0)).astype(BF16)

    locals_[2].wait()
    dn_y0().wait_recv()
    each(1, nz, lambda k: dn_y(k).wait_recv())
    out_w = dn_buf.shape[2]
    for b in range(nsp):
        at = slice(b * out_w, (b + 1) * out_w)
        res = jnp.dot(act[1 - tl], dn_buf[b], preferred_element_type=F32)
        sib_snd[:, at] = res.astype(BF16)
    sib_c().start()
    for b in range(nsp):
        at = slice(b * out_w, (b + 1) * out_w)
        part[:, at] = jnp.dot(act[tl], dn_buf[b], preferred_element_type=F32)
    sib_c().wait_recv()

    def red_step(k):
        g = lax.rem(grp + k, ng)
        rows = pl.ds(pl.multiple_of(g * share, share), share)
        red_snd[g] = (part[rows, :] + sib_buf[rows, :].astype(F32)).astype(BF16)
        red_c(k).start()

    for k in range(ng - 1, 0, -1):
        red_step(k)
    rows = pl.ds(pl.multiple_of(grp * share, share), share)
    pre[...] = part[rows, :] + sib_buf[rows, :].astype(F32) + ALPHA * h_own[...].astype(F32)
    for k in range(ng - 1, 0, -1):
        red_c(k).wait_recv()
        pre[...] += red_buf[lax.rem(grp + ng - k, ng)].astype(F32)
    out_ref[...] = layer_norm(pre[...], g2_ref[...]).astype(BF16)

    kv_y0().wait_send()
    up_y0().wait_send()
    dn_y0().wait_send()
    ow_s0().wait_send()
    h_s0().wait_send()
    sib_c().wait_send()
    for first, last, fns in (
        (1, nz, (kv_z, kv_y, up_z, up_y, dn_z, dn_y)),
        (1, nth, (ow_x, ow_s)),
        (1, ntp, (st_c, at_c)),
        (1, ng, (h_p, h_s, red_c)),
    ):
        each(first, last, lambda k: [f(k).wait_send() for f in fns])


def local(nsp, ntp, q1, q2, k1, k2, vals, lam, hg, stream, ow, g1, up, dn, g2):
    tok = q1.shape[0]
    heads = lam.shape[0]
    hv = vals.shape[1]
    vd = hv // heads
    d = ow.shape[1]
    nz, nth = nsp // 2, ntp // 2
    ng = 2 * nth
    share = tok // ntp
    fh = up.shape[1] // 2
    kv = jnp.concatenate([k1, k2, vals], axis=1)
    vm = pl.BlockSpec(memory_space=pltpu.VMEM)
    anys = pl.BlockSpec(memory_space=pl.ANY)
    sem = lambda n: pltpu.SemaphoreType.DMA((2, n))
    return pl.pallas_call(
        functools.partial(kernel, nsp, ntp, heads),
        out_shape=jax.ShapeDtypeStruct((share, d), BF16),
        in_specs=[pl.BlockSpec(memory_space=pltpu.SMEM), vm, vm, vm, vm, vm, anys, vm, anys, anys, vm],
        out_specs=vm,
        scratch_shapes=[
            pltpu.VMEM((2 * heads, tok, q1.shape[1]), BF16),
            pltpu.VMEM((2 * heads, 1, tok), F32),
            pltpu.VMEM((2 * heads, 1, tok), F32),
            pltpu.VMEM((2 * heads, vd, tok), F32),
            pltpu.VMEM((nsp,) + kv.shape, BF16),
            pltpu.VMEM((nsp, up.shape[0], fh), BF16),
            pltpu.VMEM((nsp, fh, dn.shape[1]), BF16),
            pltpu.VMEM((ntp,) + ow.shape, BF16),
            pltpu.VMEM((ntp, share, stream.shape[1]), BF16),
            pltpu.VMEM((tok, hv), BF16),
            pltpu.VMEM((ntp, share, hv), BF16),
            pltpu.VMEM((share, d), F32),
            pltpu.VMEM((share, d), BF16),
            pltpu.VMEM((2, ng, share, d), BF16),
            pltpu.VMEM((2, ng * share, fh), BF16),
            pltpu.VMEM((ng * share, d), BF16),
            pltpu.VMEM((ng * share, d), BF16),
            pltpu.VMEM((ng * share, d), F32),
            pltpu.VMEM((ng, share, d), BF16),
            pltpu.VMEM((ng, share, d), BF16),
            pltpu.SemaphoreType.DMA((3,)),
            sem(nz), sem(nz), sem(nz), sem(nz), sem(nz), sem(nz),
            sem(nth), sem(nth), sem(ntp), sem(ntp), sem(ng), sem(ng), sem(1), sem(ng),
        ],
        compiler_params=pltpu.CompilerParams(
            collective_id=0, has_side_effects=True, vmem_limit_bytes=60 * 1024 * 1024
        ),
    )(lam, q1, q2, kv, hg.reshape(1, vd), stream, ow, g1.reshape(1, d), up, dn, g2.reshape(1, d))


def solution(mesh):
    in_specs = (
        P("sp", "tp"),
        P("sp", "tp"),
        P("sp", "tp"),
        P("sp", "tp"),
        P("sp", "tp"),
        P("tp"),
        P(),
        P("sp", "tp"),
        P("tp", None),
        P(),
        P("sp", "tp"),
        P("tp", "sp"),
        P(),
    )
    body = functools.partial(local, mesh.shape["sp"], mesh.shape["tp"])
    return jax.shard_map(
        body, mesh=mesh, in_specs=in_specs, out_specs=P(("sp", "tp"), None), check_vma=False
    )
```

time: 321 us -> 117 us (0.36)
  waiting for transfers between devices: 208 us -> 0 us
  Pallas kernels: 0 us -> 113 us
  blocking collectives: 67.7 us -> 0 us
  between operations: 13.4 us -> 0.01 us
  matrix products: 12.1 us -> 0 us
  other arithmetic: 10.7 us -> 1.67 us
  local copies, waits for them, and re-layouts: 8.66 us -> 1.67 us
    all_gather x3 -> x0, waiting for transfers between devices: 147 us -> none  [the longest x1 75.1 us: local(): lax.all_gather(down_weight, 'sp', axis=1, tiled=True)]
    pallas_call x0 -> x1, Pallas kernels: none -> 113 us  [local(): pl.pallas_call(functools.partial(kernel, nsp, ntp, heads), out_shape=jax....]
    all_gather x2 -> x0, blocking collectives: 67.7 us -> none  [the longest x1 34 us: local(): lax.all_gather(key_two, 'sp', axis=0, tiled=True)]
    psum x1 -> x0, waiting for transfers between devices: 36.1 us -> none  [local(): lax.psum(lax.dynamic_update_slice_in_dim(partial_rows, own, col_start, 1)...]
    reduce_scatter x1 -> x0, waiting for transfers between devices: 23.1 us -> none  [local(): lax.psum_scatter(jnp.dot(act, down_full, preferred_element_type=jnp.float...]
    dot_general x10 -> x0, matrix products: 12.1 us -> none  [the longest x1 6.87 us: local(): jnp.dot(act, down_full, preferred_element_type=jnp.float32)]
    reduce_sum x9 -> x0, other arithmetic: 7.07 us -> none  [the longest x2 2.82 us: layer_norm(): spread = jnp.mean(jnp.square(value - centre), axis=-1, keepdims=True)]
    reshape x3 -> x0, local copies, waits for them, and re-layouts: 4.19 us -> none  [the longest x1 2.45 us: local(): keys_b = pieces[1].reshape(nblk, block, heads_local, qk_width)]
  transfers between devices with their start and end apart: 5 -> 0, of which waited for: 4 -> 0; matrix products, arithmetic and copies ran while one was open for 3% -> 0% of each run, Pallas kernels for 0% -> 0%
where the time goes in v1:
time: 117 us
  Pallas kernels  113 us (97%)
  other arithmetic  1.67 us (1%)
  local copies, waits for them, and re-layouts  1.67 us (1%)
    pallas_call x1, Pallas kernels, local(): pl.pallas_call(functools.partial(kernel, nsp, ntp, heads), out_shape=jax....  113 us

profile of v1, /device:TPU:0, one launch (start us, length us, event | category | flops | bytes accessed | tf_op | source)
XLA Modules:
  0.0 116.7 jit_solution(16106361146925009697)
XLA Ops:
  0.0 1.7 %pad_maximum_fusion.kv_ref = bf16[256,512]{1,0:T(8,128)(2,1)} fusion(bf16[256,256]{1,0:T(8,128)(2,1)} %param.17, bf16[256,128]{1,0:T(8,128)(2,1)} %param.16, bf16[256,128]{1,0:T(8,128)(2,1)} %param.15), kind=kLoop, calls=%fused_computation | loop fusion | flops 786432 | bytes 524288 | tf_op jit(solution)/shard_map/concatenate | solution.py:343
  1.7 113.4 %shard_map.127 = bf16[64,2048]{1,0:T(8,128)(2,1)} custom-call(f32[2]{0:T(128)} %lam_ref.1, bf16[256,128]{1,0:T(8,128)(2,1)} %q1_ref.1, bf16[256,128]{1,0:T(8,128)(2,1)} %q2_ref.1, bf16[256,512]{1,0:T(8,128)(2,1)} %pad_maximum_fusion.kv_ref, f32[1,128]{1,0:T(1,128)} %bitcast.5, bf16[256,512]{1,0:T(8,128)(2,1)} %st_ref.1, bf16[256,2048]{1,0:T(8,128)(2,1)} %ow_ref.1, ...), custom_call_target="tpu_custom_call" | custom-call | tf_op jit(solution)/shard_map/pallas_call | solution.py:347
  115.0 1.7 %copy.15 = bf16[64,2048]{1,0:T(8,128)(2,1)} copy(bf16[64,2048]{1,0:T(8,128)(2,1)} %shard_map.127) | data formatting | bytes 524288

commit v2 on v1

--- a/solution.py
+++ b/solution.py
@@ -23,11 +23,11 @@
 
 def kernel(
     nsp, ntp, heads,
-    lam_ref, q1_ref, q2_ref, kv_ref, hg_ref, st_ref, ow_ref, g1_ref, up_ref, dn_ref, g2_ref,
+    lam_ref, qkv_ref, hg_ref, st_ref, ow_ref, g1_ref, up_ref, dn_ref, g2_ref,
     out_ref,
-    qm, m_run, l_run, acc, kv_buf, up_buf, dn_buf, ow_buf, st_buf, at_snd, at_buf,
+    lam_all, q_buf, qm, m_run, l_run, acc, kv_buf, up_buf, dn_buf, ow_buf, st_buf, at_snd, at_buf,
     pre, h_own, h_buf, act, sib_snd, sib_buf, part, red_snd, red_buf,
-    loc_sem, kvz, kvy, upz, upy, dnz, dny, owx, ows, sts, ats, hps, hss, sbs, rds,
+    loc_sem, lms, qs, kvz, kvy, kvs, upz, upy, dnz, dny, owx, ows, sts, ats, hps, hss, sbs, rds,
 ):
     s, t = lax.axis_index("sp"), lax.axis_index("tp")
     nz, nth = nsp // 2, ntp // 2
@@ -38,18 +38,25 @@
     sib_t = th * 2 + (1 - tl)
     y_sp = z * 2 + (1 - y)
     grp = zl * nth + th
-    tok = q1_ref.shape[0]
+    tok = qkv_ref.shape[1]
     share = tok // ntp
     fh = up_ref.shape[1] // 2
-    kw = q1_ref.shape[1]
-    qk = kw // heads
     vd = acc.shape[1]
-    hv = heads * vd
+    qw = q_buf.shape[2]
+    qk = qw // 2
+    tall = q_buf.shape[1]
+    nzb = q_buf.shape[0]
     d = pre.shape[1]
-
-    def rc(src, dst, sems, i, sp, tp):
+    zq = lax.rem(z, nzb)
+    zb = z - zq
+    entry_t, head_j = zq // heads, lax.rem(zq, heads)
+    entry = tl == entry_t
+    head = th * nzb + zq
+
+    def rc(src, dst, sems, i, sp, tp, arrive=None):
+        arrive = i if arrive is None else arrive
         return pltpu.make_async_remote_copy(
-            src_ref=src, dst_ref=dst, send_sem=sems.at[0, i], recv_sem=sems.at[1, i],
+            src_ref=src, dst_ref=dst, send_sem=sems.at[0, i], recv_sem=sems.at[1, arrive],
             device_id={"sp": sp, "tp": tp}, device_id_type=MESH,
         )
 
@@ -66,16 +73,43 @@
     def zfrom(k):
         return lax.rem(z + nz - k, nz)
 
-    def kv_z(k):
-        return rc(kv_ref, kv_buf.at[s], kvz, k, zto(k) * 2 + y, t)
-
-    def kv_y0():
-        return rc(kv_ref, kv_buf.at[s], kvy, 0, y_sp, t)
+    def slab(j):
+        return qkv_ref.at[j, :, pl.ds(qw, qw + vd)]
+
+    def q_c(j, hf):
+        zd = zb + heads * tl + j
+        return rc(
+            qkv_ref.at[j, pl.ds(hf * tall, tall), pl.ds(0, qw)], q_buf.at[zq],
+            qs, j * 2 + hf, zd * 2 + y, th * 2 + hf, zq,
+        )
+
+    def q_in(i):
+        return rc(q_buf.at[i], q_buf.at[i], qs, 0, y_sp, t, i)
+
+    def kv_z(j, r):
+        zd = r * nzb + heads * tl + j
+        return rc(
+            slab(j), kv_buf.at[s], kvz, r * heads + j, zd * 2 + y, t, lax.rem(zd - z + nz, nz)
+        )
+
+    def kv_zin(k):
+        b = zfrom(k) * 2 + y
+        return rc(kv_buf.at[b], kv_buf.at[b], kvz, 0, y_sp, t, k)
 
     def kv_y(k):
         b = zfrom(k) * 2 + y
         return rc(kv_buf.at[b], kv_buf.at[b], kvy, k, y_sp, t)
 
+    def kv_y0():
+        return rc(slab(head_j), kv_buf.at[s], kvy, 0, y_sp, t)
+
+    def kv_s(k, side):
+        b = zfrom(k) * 2 + lax.rem(y + side, 2)
+        return rc(kv_buf.at[b], kv_buf.at[b], kvs, side * nz + k, s, sib_t)
+
+    def kv_s0():
+        return rc(slab(head_j), kv_buf.at[s], kvs, 0, s, sib_t)
+
     def up_half(j):
         return up_ref.at[:, pl.ds(pl.multiple_of(j * fh, fh), fh)]
 
@@ -121,9 +155,22 @@
         td = lax.rem(t + k, ntp)
         return rc(st_ref.at[rows_of(td), :], st_buf.at[t], sts, k, s, td)
 
-    def at_c(k):
-        td = lax.rem(t + k, ntp)
-        return rc(at_snd.at[rows_of(td), :], at_buf.at[t], ats, k, s, td)
+    def at_c(i, u):
+        rows = pl.ds(i * tall + u * share, share)
+        cols = pl.ds(pl.multiple_of(head * vd, vd), vd)
+        return rc(
+            at_snd.at[rows, :], at_buf.at[:, cols], ats, i * nth + u,
+            (zb + i) * 2 + y, tl * nth + u, head,
+        )
+
+    def at_in(hd):
+        ref = at_buf.at[:, pl.ds(hd * vd, vd)]
+        return rc(ref, ref, ats, 0, y_sp, t, hd)
+
+    mine = t // nth == tl
+
+    def at_self(hd):
+        return mine & (head == hd)
 
     def grp_dev(g):
         return (zh * 2 + g // nth) * 2 + y, lax.rem(g, nth) * 2 + tl
@@ -152,14 +199,43 @@
     def greet(sp, tp):
         pl.semaphore_signal(barrier, inc=1, device_id={"sp": sp, "tp": tp}, device_id_type=MESH)
 
-    each(1, nz, lambda k: greet(zto(k) * 2 + y, t))
+    for i in range(nzb):
+        for tt in range(ntp):
+            pl.when((i != zq) | (tt != t))(functools.partial(greet, (zb + i) * 2 + y, tt))
+    if nz > nzb:
+        each(0, nz, lambda k: pl.when((k < zb) | (k >= zb + nzb))(lambda: greet(k * 2 + y, t)))
     greet(y_sp, t)
-    each(1, ntp, lambda k: greet(s, lax.rem(t + k, ntp)))
-    each(1, nth, lambda k: greet((zh * 2 + 1 - zl) * 2 + y, lax.rem(th + k, nth) * 2 + tl))
-    pl.semaphore_wait(barrier, (nz - 1) + 1 + (ntp - 1) + (nth - 1))
-
-    each(1, nz, lambda k: kv_z(k).start())
-    kv_y0().start()
+    pl.semaphore_wait(barrier, nzb * ntp - 1 + nz - nzb + 1)
+
+    def q_self(j, hf):
+        return (zq == heads * tl + j) & (hf == tl)
+
+    pairs = [(j, hf) for j in range(heads) for hf in range(2)]
+    for j, hf in pairs:
+        pl.when(jnp.logical_not(q_self(j, hf)))(lambda: q_c(j, hf).start())
+
+        @pl.when(q_self(j, hf))
+        def _():
+            q_buf[zq] = qkv_ref[j, hf * tall : (hf + 1) * tall, :qw]
+
+    def lam_c():
+        return rc(lam_ref, lam_all.at[tl], lms, 0, s, sib_t)
+
+    lam_all[tl] = lam_ref[...]
+
+    def kv_out(fn):
+        for j in range(heads):
+            each(0, nz // nzb, lambda r: pl.when(r * nzb + heads * tl + j != z)(lambda: fn(kv_z(j, r))))
+
+    kv_out(lambda c: c.start())
+
+    @pl.when(entry)
+    def _():
+        kv_y0().start()
+        kv_s0().start()
+        kv_buf[s] = qkv_ref[head_j, :, qw:]
+
+    lam_c().start()
     each(1, ntp, lambda k: st_c(k).start())
     each(1, nth, lambda k: ow_x(k).start())
     ow_s0().start()
@@ -171,42 +247,47 @@
     for c in locals_:
         c.start()
     each(1, nz, lambda k: up_z(k).start())
-    each(1, nz, lambda k: dn_z(k).start())
 
     scale = qk ** (-0.5)
-    lane = lax.broadcasted_iota(jnp.int32, (tok, kw), 1)
-    for i, q_ref in enumerate((q1_ref, q2_ref)):
-        qv = q_ref[...].astype(F32) * scale
-        for h in range(heads):
-            keep = (lane >= h * qk) & (lane < (h + 1) * qk)
-            qm[i * heads + h] = jnp.where(keep, qv, 0.0).astype(BF16)
     m_run[...] = jnp.full(m_run.shape, -1e30, F32)
     l_run[...] = jnp.zeros(l_run.shape, F32)
     acc[...] = jnp.zeros(acc.shape, F32)
+    lane = lax.broadcasted_iota(jnp.int32, (tall, qw), 1)
+    for i in range(nzb):
+        pl.when(jnp.logical_not((zq == i) & entry))(lambda: q_in(i).wait_recv())
+        qv = q_buf[i].astype(F32) * scale
+        for mp in range(2):
+            keep = (lane >= mp * qk) & (lane < (mp + 1) * qk)
+            qm[mp, i * tall : (i + 1) * tall, :] = jnp.where(keep, qv, 0.0).astype(BF16)
 
     def absorb(block):
-        for h in range(heads):
-            v = block[:, 2 * kw + h * vd : 2 * kw + (h + 1) * vd]
-            for i in range(2):
-                r = i * heads + h
-                sc = lax.dot_general(
-                    block[:, i * kw : (i + 1) * kw], qm[r], NT, preferred_element_type=F32
-                )
-                old = m_run[r]
-                new = jnp.maximum(old, jnp.max(sc, axis=0, keepdims=True))
-                fac = jnp.exp(old - new)
-                ex = jnp.exp(sc - new)
-                l_run[r] = l_run[r] * fac + jnp.sum(ex, axis=0, keepdims=True)
-                acc[r] = acc[r] * fac + lax.dot_general(
-                    v, ex.astype(BF16), TN, preferred_element_type=F32
-                )
-                m_run[r] = new
-
-    absorb(kv_ref)
+        v = block[:, qw:]
+        for r in range(2):
+            sc = lax.dot_general(block[:, :qw], qm[r], NT, preferred_element_type=F32)
+            old = m_run[r]
+            new = jnp.maximum(old, jnp.max(sc, axis=0, keepdims=True))
+            fac = jnp.exp(old - new)
+            ex = jnp.exp(sc - new)
+            l_run[r] = l_run[r] * fac + jnp.sum(ex, axis=0, keepdims=True)
+            acc[r] = acc[r] * fac + lax.dot_general(
+                v, ex.astype(BF16), TN, preferred_element_type=F32
+            )
+            m_run[r] = new
+
+    def own_step():
+        pl.when(jnp.logical_not(entry))(lambda: kv_s0().wait_recv())
+        absorb(kv_buf.at[s])
+
+    own_step()
 
     def z_step(k, c):
-        kv_z(k).wait_recv()
-        kv_y(k).start()
+        @pl.when(entry)
+        def _():
+            kv_zin(k).wait_recv()
+            kv_y(k).start()
+            kv_s(k, 0).start()
+
+        pl.when(jnp.logical_not(entry))(lambda: kv_s(k, 0).wait_recv())
         absorb(kv_buf.at[zfrom(k) * 2 + y])
         return c
 
@@ -215,26 +296,42 @@
     dn_y0().start()
 
     def y_step(k, c):
-        kv_y(k).wait_recv()
+        @pl.when(entry)
+        def _():
+            kv_y(k).wait_recv()
+            kv_s(k, 1).start()
+
+        pl.when(jnp.logical_not(entry))(lambda: kv_s(k, 1).wait_recv())
         absorb(kv_buf.at[zfrom(k) * 2 + 1 - y])
         return c
 
     lax.fori_loop(0, nz, y_step, 0)
+    up_z(1).wait_recv()
+    up_y(1).start()
 
     for k in range(1, nth):
         ow_x(k).wait_recv()
         ow_s(k).start()
 
-    for h in range(heads):
-        mixed = acc[h] / l_run[h] - lam_ref[h] * (acc[heads + h] / l_run[heads + h])
-        inv = lax.rsqrt(jnp.mean(jnp.square(mixed), axis=0, keepdims=True) + 1e-05)
-        normed = jnp.transpose(mixed * inv) * hg_ref[...] * 0.8
-        at_snd[:, h * vd : (h + 1) * vd] = normed.astype(BF16)
-    each(1, ntp, lambda k: at_c(k).start())
-    at_buf[t] = at_snd[rows_of(t), :]
+    lam_c().wait_recv()
+    lam = lam_all[entry_t, head_j][:, :1]
+    mixed = acc[0] / l_run[0] - lam * (acc[1] / l_run[1])
+    inv = lax.rsqrt(jnp.mean(jnp.square(mixed), axis=0, keepdims=True) + 1e-05)
+    normed = jnp.transpose(mixed * inv) * hg_ref[...] * 0.8
+    at_snd[...] = normed.astype(BF16)
+    spots = [(i, u) for i in range(nzb) for u in range(nth)]
+    for i, u in spots:
+        own = (zq == i) & (tl * nth + u == t)
+        pl.when(jnp.logical_not(own))(lambda: at_c(i, u).start())
+
+        @pl.when(own)
+        def _():
+            cols = pl.ds(pl.multiple_of(head * vd, vd), vd)
+            at_buf[:, cols] = at_snd[i * tall + u * share : i * tall + (u + 1) * share, :]
+
     st_buf[t] = st_ref[rows_of(t), :]
-    up_z(1).wait_recv()
-    up_y(1).start()
+    up_z(2).wait_recv()
+    up_y(2).start()
 
     each(1, ntp, lambda k: st_c(k).wait_recv())
     cols = st_ref.shape[1]
@@ -244,31 +341,34 @@
     ow_s0().wait_recv()
     for k in range(1, nth):
         ow_s(k).wait_recv()
-    each(1, ntp, lambda k: at_c(k).wait_recv())
+    for hd in range(nzb * nth):
+        pl.when(jnp.logical_not(at_self(hd)))(lambda: at_in(hd).wait_recv())
     for b in range(ntp):
-        pre[...] += jnp.dot(at_buf[b], ow_buf[b], preferred_element_type=F32)
+        at = slice(b * cols, (b + 1) * cols)
+        full = ow_buf[:, :, at].reshape(at_buf.shape[1], cols)
+        pre[:, at] += jnp.dot(at_buf[...], full, preferred_element_type=F32)
     h_own[...] = layer_norm(pre[...], g1_ref[...]).astype(BF16)
     each(1, ng, lambda k: h_p(k).start())
     h_s0().start()
+    each(1, nz, lambda k: dn_z(k).start())
     h_buf[tl, grp] = h_own[...]
 
     def up_fwd(k):
         up_z(k).wait_recv()
         up_y(k).start()
 
-    each(2, nz, up_fwd)
+    each(3, nz, up_fwd)
 
     def h_fwd(k):
         h_p(k).wait_recv()
         h_s(k).start()
 
-    each(1, ng, h_fwd)
-
     def dn_fwd(k):
         dn_z(k).wait_recv()
         dn_y(k).start()
 
-    each(1, nz, dn_fwd)
+    each(1, ng, h_fwd)
+    dn_fwd(1)
     h_s0().wait_recv()
     each(1, ng, lambda k: h_s(k).wait_recv())
     locals_[1].wait()
@@ -286,6 +386,7 @@
             up = jnp.dot(hid, w, preferred_element_type=F32)
             act[side, :, at] = jnp.square(jnp.maximum(up, 0.0)).astype(BF16)
 
+    each(2, nz, dn_fwd)
     locals_[2].wait()
     dn_y0().wait_recv()
     each(1, nz, lambda k: dn_y(k).wait_recv())
@@ -315,16 +416,31 @@
         pre[...] += red_buf[lax.rem(grp + ng - k, ng)].astype(F32)
     out_ref[...] = layer_norm(pre[...], g2_ref[...]).astype(BF16)
 
-    kv_y0().wait_send()
+    for j, hf in pairs:
+        pl.when(jnp.logical_not(q_self(j, hf)))(lambda: q_c(j, hf).wait_send())
+    for i, u in spots:
+        own = (zq == i) & (tl * nth + u == t)
+        pl.when(jnp.logical_not(own))(lambda: at_c(i, u).wait_send())
+    kv_out(lambda c: c.wait_send())
+
+    @pl.when(entry)
+    def _():
+        kv_y0().wait_send()
+        kv_s0().wait_send()
+        each(1, nz, lambda k: kv_y(k).wait_send())
+        each(1, nz, lambda k: kv_s(k, 0).wait_send())
+        each(0, nz, lambda k: kv_s(k, 1).wait_send())
+
+    lam_c().wait_send()
     up_y0().wait_send()
     dn_y0().wait_send()
     ow_s0().wait_send()
     h_s0().wait_send()
     sib_c().wait_send()
     for first, last, fns in (
-        (1, nz, (kv_z, kv_y, up_z, up_y, dn_z, dn_y)),
+        (1, nz, (up_z, up_y, dn_z, dn_y)),
         (1, nth, (ow_x, ow_s)),
-        (1, ntp, (st_c, at_c)),
+        (1, ntp, (st_c,)),
         (1, ng, (h_p, h_s, red_c)),
     ):
         each(first, last, lambda k: [f(k).wait_send() for f in fns])
@@ -340,27 +456,33 @@
     ng = 2 * nth
     share = tok // ntp
     fh = up.shape[1] // 2
-    kv = jnp.concatenate([k1, k2, vals], axis=1)
+    qk = q1.shape[1] // heads
+    parts = [a.reshape(tok, heads, -1) for a in (q1, q2, k1, k2, vals)]
+    qkv = jnp.concatenate(parts, axis=2).transpose(1, 0, 2)
+    nzb, tall = 2 * heads, nth * share
+    lam = jnp.broadcast_to(lam[:, None, None], (heads, 1, 128))
     vm = pl.BlockSpec(memory_space=pltpu.VMEM)
     anys = pl.BlockSpec(memory_space=pl.ANY)
     sem = lambda n: pltpu.SemaphoreType.DMA((2, n))
     return pl.pallas_call(
         functools.partial(kernel, nsp, ntp, heads),
         out_shape=jax.ShapeDtypeStruct((share, d), BF16),
-        in_specs=[pl.BlockSpec(memory_space=pltpu.SMEM), vm, vm, vm, vm, vm, anys, vm, anys, anys, vm],
+        in_specs=[vm, vm, vm, vm, anys, vm, anys, anys, vm],
         out_specs=vm,
         scratch_shapes=[
-            pltpu.VMEM((2 * heads, tok, q1.shape[1]), BF16),
-            pltpu.VMEM((2 * heads, 1, tok), F32),
-            pltpu.VMEM((2 * heads, 1, tok), F32),
-            pltpu.VMEM((2 * heads, vd, tok), F32),
-            pltpu.VMEM((nsp,) + kv.shape, BF16),
+            pltpu.VMEM((2,) + lam.shape, F32),
+            pltpu.VMEM((nzb, tall, 2 * qk), BF16),
+            pltpu.VMEM((2, nzb * tall, 2 * qk), BF16),
+            pltpu.VMEM((2, 1, nzb * tall), F32),
+            pltpu.VMEM((2, 1, nzb * tall), F32),
+            pltpu.VMEM((2, vd, nzb * tall), F32),
+            pltpu.VMEM((nsp, tok, 2 * qk + vd), BF16),
             pltpu.VMEM((nsp, up.shape[0], fh), BF16),
             pltpu.VMEM((nsp, fh, dn.shape[1]), BF16),
             pltpu.VMEM((ntp,) + ow.shape, BF16),
             pltpu.VMEM((ntp, share, stream.shape[1]), BF16),
-            pltpu.VMEM((tok, hv), BF16),
-            pltpu.VMEM((ntp, share, hv), BF16),
+            pltpu.VMEM((nzb * tall, vd), BF16),
+            pltpu.VMEM((share, ntp * hv), BF16),
             pltpu.VMEM((share, d), F32),
             pltpu.VMEM((share, d), BF16),
             pltpu.VMEM((2, ng, share, d), BF16),
@@ -371,13 +493,14 @@
             pltpu.VMEM((ng, share, d), BF16),
             pltpu.VMEM((ng, share, d), BF16),
             pltpu.SemaphoreType.DMA((3,)),
-            sem(nz), sem(nz), sem(nz), sem(nz), sem(nz), sem(nz),
-            sem(nth), sem(nth), sem(ntp), sem(ntp), sem(ng), sem(ng), sem(1), sem(ng),
+            sem(1),
+            sem(max(2 * heads, nzb)), sem(nz), sem(nz), sem(2 * nz), sem(nz), sem(nz), sem(nz), sem(nz),
+            sem(nth), sem(nth), sem(ntp), sem(max(nzb * nth, nzb * nth)), sem(ng), sem(ng), sem(1), sem(ng),
         ],
         compiler_params=pltpu.CompilerParams(
             collective_id=0, has_side_effects=True, vmem_limit_bytes=60 * 1024 * 1024
         ),
-    )(lam, q1, q2, kv, hg.reshape(1, vd), stream, ow, g1.reshape(1, d), up, dn, g2.reshape(1, d))
+    )(lam, qkv, hg.reshape(1, vd), stream, ow, g1.reshape(1, d), up, dn, g2.reshape(1, d))
 
 
 def solution(mesh):

time: 117 us -> 114 us (0.974)
  Pallas kernels: 113 us -> 105 us
  local copies, waits for them, and re-layouts: 1.67 us -> 8.82 us
  other arithmetic: 1.67 us -> 0 us
    pallas_call x1, Pallas kernels: 113 us -> 105 us  [local(): pl.pallas_call(functools.partial(kernel, nsp, ntp, heads), out_shape=jax....]
    unnamed x1 -> x16, local copies, waits for them, and re-layouts: 1.67 us -> 6.59 us
    concatenate x1 -> x0, other arithmetic: 1.67 us -> none  [local(): kv = jnp.concatenate([k1, k2, vals], axis=1)]
where the time goes in v2:
time: 114 us
  Pallas kernels  105 us (92%)
  local copies, waits for them, and re-layouts  8.82 us (8%)
    pallas_call x1, Pallas kernels, local(): pl.pallas_call(functools.partial(kernel, nsp, ntp, heads), out_shape=jax....  105 us
    unnamed x16, local copies, waits for them, and re-layouts  6.59 us

profile of v2, /device:TPU:0, one launch (start us, length us, event | category | flops | bytes accessed | tf_op | source)
XLA Modules:
  0.0 114.0 jit_solution(5069914157509646557)
XLA Ops:
  0.0 1.0 copy.18
  1.0 0.0 copy-start
  1.0 0.1 copy.23
  1.1 0.7 copy-done
  1.9 0.1 copy.14
  2.0 0.0 copy-start.1
  2.0 0.1 copy.19
  2.1 0.7 copy-done.1
  2.8 0.1 copy.15
  2.9 0.0 copy-start.2
  2.9 0.1 copy.20
  3.1 0.7 copy-done.2
  3.8 0.1 copy.16
  3.9 0.0 copy-start.3
  3.9 0.1 copy.21
  4.0 0.7 copy-done.3
  4.7 0.1 copy.17
  4.8 0.1 copy.22
  5.0 1.0 concatenate.3
  6.0 0.0 copy-start.4
  6.0 0.7 copy-done.4
  6.6 0.6 broadcast_in_dim.2.lam_ref
  7.2 105.1 %shard_map.127 = bf16[64,2048]{1,0:T(8,128)(2,1)} custom-call(f32[2,1,128]{2,1,0:T(1,128)} %broadcast_in_dim.2.lam_ref, bf16[2,256,384]{2,1,0:T(8,128)(2,1)} %bitcast.9, f32[1,128]{1,0:T(1,128)} %bitcast.17, bf16[256,512]{1,0:T(8,128)(2,1)} %st_ref.1, bf16[256,2048]{1,0:T(8,128)(2,1)} %ow_ref.1, f32[1,2048]{1,0:T(1,128)} %bitcast.15, ...), custom_call_target="tpu_custom_call" | custom-call | tf_op jit(solution)/shard_map/pallas_call | solution.py:467
  112.3 1.7 %copy.25 = bf16[64,2048]{1,0:T(8,128)(2,1)} copy(bf16[64,2048]{1,0:T(8,128)(2,1)} %shard_map.127) | data formatting | bytes 524288
Async XLA Ops:
  1.0 0.8 copy-start
  2.0 0.8 copy-start.1
  2.9 0.8 copy-start.2
  3.9 0.8 copy-start.3
  6.0 0.7 copy-start.4
